TPU v7x, 32 devices: a whole 2x2x4 slice. The times are simulated.
32 devices in a mesh: tp: 8 (over z, x), dp: 4 (over y, core).
Axes of the slice: x: 2, y: 2, z: 4, core: 2. Of those that a mesh axis runs over, the one named last changes fastest.
Arguments:
- tokens: bfloat16 [64, 4096], P(None, 'dp'), may hold values from -6 to 6
- recurrent_state: float32 [2, 64, 262144], P(None, 'dp', 'tp'), may hold values from -24 to 24
- pre_gain: float32 [2, 4096], P(None, 'dp'), may hold values from 0.1 to 1.9
- w_query: bfloat16 [2, 4096, 2048], P(None, 'dp', 'tp'), may hold values from -0.09375 to 0.09375
- w_key: bfloat16 [2, 4096, 2048], P(None, 'dp', 'tp'), may hold values from -0.09375 to 0.09375
- w_value: bfloat16 [2, 4096, 4096], P(None, 'dp', 'tp'), may hold values from -0.09375 to 0.09375
- w_gate: bfloat16 [2, 4096, 4096], P(None, 'dp', 'tp'), may hold values from -0.09375 to 0.09375
- w_decay: bfloat16 [2, 4096, 2048], P(None, 'dp', 'tp'), may hold values from -1 to 1
- decay_bias: float32 [2, 2048], P(None, 'tp'), may hold values from -5 to 3
- head_gain: float32 [2, 128], replicated, may hold values from 0.1 to 1.9
- w_out: bfloat16 [2, 4096, 4096], P(None, 'tp', 'dp'), may hold values from -0.09375 to 0.09375
- post_gain: float32 [2, 4096], P(None, 'dp'), may hold values from 0.1 to 1.9
Outputs:
- hidden_out: bfloat16 [64, 4096], P(None, 'dp')
- state_out: float32 [2, 64, 262144], P(None, 'dp', 'tp')
All inputs are finite; a program needn't handle non-finite values.
Results may differ from a plain program's by a relative error of at most 0.015.
Values may be sent and summed in bfloat16 or wider, within the bound.
A program may use at most 64 MiB of HBM per device.

v0:
```python
import jax
import jax.numpy as jnp
from jax import lax
from jax.sharding import PartitionSpec as P

D = 4096
KEY = 64
VAL = 128
epsilon = 1e-06


def local(
    tokens,
    recurrent_state,
    pre_gain,
    w_query,
    w_key,
    w_value,
    w_gate,
    w_decay,
    decay_bias,
    head_gain,
    w_out,
    post_gain,
):
    local_seqs = recurrent_state.shape[1]
    value_cols = recurrent_state.shape[2] // KEY
    heads_here = value_cols // VAL
    highest = lax.Precision.HIGHEST
    spread = (
        jnp.arange(value_cols, dtype=jnp.int32)[None, :] // VAL
        == jnp.arange(heads_here, dtype=jnp.int32)[:, None]
    ).astype(jnp.float32)

    def spread_heads(vectors):
        shaped = vectors.astype(jnp.float32).reshape(local_seqs, heads_here, KEY)
        return jnp.einsum("bhk,hc->bck", shaped, spread, precision=highest)

    residual = tokens
    new_states = []
    for section_index in range(2):
        wide_float = residual.astype(jnp.float32)
        squares_part = jnp.sum(wide_float * wide_float, axis=1)
        normed = (wide_float * pre_gain[section_index]).astype(jnp.bfloat16)
        partials = tuple(
            (
                jnp.dot(normed, weights[section_index], preferred_element_type=jnp.float32)
                for weights in (w_query, w_key, w_value, w_gate, w_decay)
            )
        )
        summed = lax.psum_scatter(partials + (squares_part,), "dp", scatter_dimension=0, tiled=True)
        projected = summed[:5]
        own_squares = summed[5]
        row_scale = lax.rsqrt(own_squares / D + epsilon)[:, None]
        query_part = (projected[0] * row_scale).astype(jnp.bfloat16)
        key_part = (projected[1] * row_scale).astype(jnp.bfloat16)
        values_own = projected[2] * row_scale
        gate_pre = projected[3] * row_scale
        log_decay = jax.nn.log_sigmoid(projected[4] * row_scale + decay_bias[section_index]) / 16.0
        query_cols = spread_heads(query_part)
        key_cols = spread_heads(key_part)
        decay_cols = jnp.exp(spread_heads(log_decay))
        old_state = recurrent_state[section_index].reshape(local_seqs, value_cols, KEY)
        new_state = decay_cols * old_state + key_cols * values_own[:, :, None]
        readout = jnp.sum(query_cols * new_state, axis=2) * KEY ** (-0.5)
        head_mean = jnp.mean(
            (readout * readout).reshape(local_seqs, heads_here, VAL), axis=2, keepdims=True
        )
        scaled = (
            readout.reshape(local_seqs, heads_here, VAL)
            * lax.rsqrt(head_mean + epsilon)
            * head_gain[section_index]
        )
        mixed = (scaled.reshape(local_seqs, value_cols) * jax.nn.silu(gate_pre)).astype(
            jnp.bfloat16
        )
        out_weight = w_out[section_index]
        partial_out = jnp.dot(
            lax.all_gather(mixed, "dp", axis=0, tiled=True),
            out_weight,
            preferred_element_type=jnp.float32,
        )
        out_rows = lax.psum(partial_out, "tp")
        out_squares = lax.psum(jnp.sum(out_rows * out_rows, axis=1), "dp")
        residual = (
            wide_float
            + out_rows * lax.rsqrt(out_squares / D + epsilon)[:, None] * post_gain[section_index]
        ).astype(jnp.bfloat16)
        new_states.append(new_state.reshape(local_seqs, value_cols * KEY))
    return (residual, jnp.stack(new_states))


def solution(mesh):
    in_specs = (
        P(None, "dp"),
        P(None, "dp", "tp"),
        P(None, "dp"),
        P(None, "dp", "tp"),
        P(None, "dp", "tp"),
        P(None, "dp", "tp"),
        P(None, "dp", "tp"),
        P(None, "dp", "tp"),
        P(None, "tp"),
        P(),
        P(None, "tp", "dp"),
        P(None, "dp"),
    )
    out_specs = (P(None, "dp"), P(None, "dp", "tp"))
    return jax.shard_map(local, mesh=mesh, in_specs=in_specs, out_specs=out_specs, check_vma=False)
```

profile of v0, /device:TPU:0, one launch (start us, length us, event | category | flops | bytes accessed | tf_op | source)
XLA Modules:
  0.0 412.4 jit_solution(11796743993679151280)
XLA Ops:
  17.6 3.9 fusion.83
  21.5 3.0 reshape_squeeze.6
  24.5 3.8 copy.18
  28.3 8.4 %all-reduce = f32[64]{0:T(128)S(1)} all-reduce(f32[64]{0:T(128)S(1)} %fusion.41), channel_id=3, replica_groups=mesh['tp'=8,'dp'=4] {'dp'}, use_global_device_ids=true, to_apply=%region_2.3.clone | all-reduce | flops 64 | bytes 512
  38.1 16.7 %reduce-scatter.13.cloned.1.call-done = f32[16,256]{1,0:T(8,128)} async-done(((f32[64,256]{1,0:T(8,128)}), f32[16,256]{1,0:T(8,128)}) %reduce-scatter.13.cloned.1.call-update) | async-done | bytes 16400 | tf_op jit(solution)/shard_map/reduce_scatter | solution.py:51
  54.7 22.0 %reduce-scatter.15.cloned.1.call-done = f32[16,256]{1,0:T(8,128)} async-done(((f32[64,256]{1,0:T(8,128)}), f32[16,256]{1,0:T(8,128)}) %reduce-scatter.15.cloned.1.call-update) | async-done | bytes 16400 | tf_op jit(solution)/shard_map/reduce_scatter | solution.py:51
  77.8 2.4 fusion.79
  80.2 19.1 %reduce-scatter.17.cloned.1.call-done = f32[16,512]{1,0:T(8,128)} async-done(((f32[64,512]{1,0:T(8,128)}), f32[16,512]{1,0:T(8,128)}) %reduce-scatter.17.cloned.1.call-update) | async-done | bytes 32784 | tf_op jit(solution)/shard_map/reduce_scatter | solution.py:51
  100.1 2.7 fusion.2
  103.5 17.7 %reduce-scatter.19.cloned.1.call-done = f32[16,512]{1,0:T(8,128)} async-done(((f32[64,512]{1,0:T(8,128)}), f32[16,512]{1,0:T(8,128)}) %reduce-scatter.19.cloned.1.call-update) | async-done | bytes 32784 | tf_op jit(solution)/shard_map/reduce_scatter | solution.py:51
  122.2 5.2 %all_gather.6 = bf16[64,512]{1,0:T(8,128)(2,1)S(1)} all-gather(bf16[16,512]{1,0:T(8,128)(2,1)S(1)} %fusion.61), channel_id=1, replica_groups=mesh['tp'=8,'dp'=4] {'dp'}, dimensions={0}, use_global_device_ids=true | all-gather | bytes 81920 | tf_op jit(solution)/shard_map/all_gather | solution.py:79
  129.7 4.2 %reshape_squeeze.7 = f32[16,512,64]{2,1,0:T(8,128)} reshape(f32[1,16,32768]{2,1,0:T(8,128)} %get-tuple-element.4) | data formatting | bytes 4194304 | tf_op jit(solution)/shard_map/reshape;squeeze | solution.py:63
  133.9 3.9 copy.19
  137.8 2.8 copy.20
  140.6 4.1 stack_reshape.6
  144.7 56.1 %all-reduce.5.cloned.1.call-done = f32[64,1024]{1,0:T(8,128)} async-done(((f32[64,1024]{1,0:T(8,128)}), f32[64,1024]{1,0:T(8,128)}) %all-reduce.5.cloned.1.call-update) | async-done | bytes 262160 | tf_op jit(solution)/shard_map/psum | solution.py:83
  201.9 5.7 %psum.29 = f32[64]{0:T(128)S(1)} all-reduce(f32[64]{0:T(128)S(1)} %multiply_reduce_fusion.1), channel_id=1, replica_groups=mesh['tp'=8,'dp'=4] {'dp'}, use_global_device_ids=true, to_apply=%region_11.12 | all-reduce | flops 64 | bytes 512 | tf_op jit(solution)/shard_map/psum | solution.py:84
  209.7 6.6 %all-reduce.1 = f32[64]{0:T(128)S(1)} all-reduce(f32[64]{0:T(128)S(1)} %get-tuple-element.2), channel_id=9, replica_groups=mesh['tp'=8,'dp'=4] {'dp'}, use_global_device_ids=true, to_apply=%region_14.15.clone | all-reduce | flops 64 | bytes 512
  223.7 5.1 %reduce-scatter.21.cloned.1.call-done = f32[16,256]{1,0:T(8,128)} async-done(((f32[64,256]{1,0:T(8,128)}), f32[16,256]{1,0:T(8,128)}) %reduce-scatter.21.cloned.1.call-update) | async-done | bytes 16400 | tf_op jit(solution)/shard_map/reduce_scatter | solution.py:51
  228.8 22.0 %reduce-scatter.23.cloned.1.call-done = f32[16,256]{1,0:T(8,128)} async-done(((f32[64,256]{1,0:T(8,128)}), f32[16,256]{1,0:T(8,128)}) %reduce-scatter.23.cloned.1.call-update) | async-done | bytes 16400 | tf_op jit(solution)/shard_map/reduce_scatter | solution.py:51
  250.8 22.0 %reduce-scatter.25.cloned.1.call-done = f32[16,256]{1,0:T(8,128)} async-done(((f32[64,256]{1,0:T(8,128)}), f32[16,256]{1,0:T(8,128)}) %reduce-scatter.25.cloned.1.call-update) | async-done | bytes 16400 | tf_op jit(solution)/shard_map/reduce_scatter | solution.py:51
  273.7 2.4 fusion.75
  276.3 19.1 %reduce-scatter.27.cloned.1.call-done = f32[16,512]{1,0:T(8,128)} async-done(((f32[64,512]{1,0:T(8,128)}), f32[16,512]{1,0:T(8,128)}) %reduce-scatter.27.cloned.1.call-update) | async-done | bytes 32784 | tf_op jit(solution)/shard_map/reduce_scatter | solution.py:51
  296.2 2.8 fusion
  299.4 2.8 copy.21
  302.3 15.1 %reduce-scatter.29.cloned.1.call-done = f32[16,512]{1,0:T(8,128)} async-done(((f32[64,512]{1,0:T(8,128)}), f32[16,512]{1,0:T(8,128)}) %reduce-scatter.29.cloned.1.call-update) | async-done | bytes 32784 | tf_op jit(solution)/shard_map/reduce_scatter | solution.py:51
  318.3 5.2 %all_gather.7 = bf16[64,512]{1,0:T(8,128)(2,1)S(1)} all-gather(bf16[16,512]{1,0:T(8,128)(2,1)S(1)} %fusion.58), channel_id=1, replica_groups=mesh['tp'=8,'dp'=4] {'dp'}, dimensions={0}, use_global_device_ids=true | all-gather | bytes 81920 | tf_op jit(solution)/shard_map/all_gather | solution.py:79
  323.6 2.2 fusion.4
  325.8 4.0 stack_reshape.7
  329.9 3.9 pad_maximum_fusion
  333.7 63.3 %all-reduce.7.cloned.1.call-done = f32[64,1024]{1,0:T(8,128)} async-done(((f32[64,1024]{1,0:T(8,128)}), f32[64,1024]{1,0:T(8,128)}) %all-reduce.7.cloned.1.call-update) | async-done | bytes 262160 | tf_op jit(solution)/shard_map/psum | solution.py:83
  398.1 5.7 %psum.31 = f32[64]{0:T(128)S(1)} all-reduce(f32[64]{0:T(128)S(1)} %multiply_reduce_fusion), channel_id=1, replica_groups=mesh['tp'=8,'dp'=4] {'dp'}, use_global_device_ids=true, to_apply=%region_23.24 | all-reduce | flops 64 | bytes 512 | tf_op jit(solution)/shard_map/psum | solution.py:84
  (95 shorter events, 33.6 us)
Async XLA Ops:
  7.2 7.0 %copy-start.1 = (bf16[64,1024]{1,0:T(8,128)(2,1)S(1)}, bf16[64,1024]{1,0:T(8,128)(2,1)}, u32[]{:S(2)}) copy-start(bf16[64,1024]{1,0:T(8,128)(2,1)} %param.12) | copy-start | bytes 393220
  7.2 7.0 %copy-start.5 = (bf16[2,1024,512]{2,1,0:T(8,128)(2,1)S(1)}, bf16[2,1024,512]{2,1,0:T(8,128)(2,1)}, u32[]{:S(2)}) copy-start(bf16[2,1024,512]{2,1,0:T(8,128)(2,1)} %param.17) | copy-start | bytes 6291460
  7.2 30.9 %reduce-scatter.11.cloned.1.call-start = ((), (), s32[]{:S(2)}) async-start(), calls=%async_computation.10 | async-start | bytes 81920 | tf_op jit(solution)/shard_map/reduce_scatter | solution.py:51
  10.1 44.6 %reduce-scatter.13.cloned.1.call-start = ((), (), s32[]{:S(2)}) async-start(), calls=%async_computation.11 | async-start | bytes 81920 | tf_op jit(solution)/shard_map/reduce_scatter | solution.py:51
  12.1 64.6 %reduce-scatter.15.cloned.1.call-start = ((), (), s32[]{:S(2)}) async-start(), calls=%async_computation.12 | async-start | bytes 81920 | tf_op jit(solution)/shard_map/reduce_scatter | solution.py:51
  14.1 85.1 %reduce-scatter.17.cloned.1.call-start = ((), (), s32[]{:S(2)}) async-start(), calls=%async_computation.13 | async-start | bytes 163840 | tf_op jit(solution)/shard_map/reduce_scatter | solution.py:51
  15.2 106.0 %reduce-scatter.19.cloned.1.call-start = ((), (), s32[]{:S(2)}) async-start(), calls=%async_computation.14 | async-start | bytes 163840 | tf_op jit(solution)/shard_map/reduce_scatter | solution.py:51
  17.4 183.4 %all-reduce.5.cloned.1.call-start = ((), (), s32[]{:S(2)}) async-start(), calls=%async_computation.15 | async-start | bytes 524288 | tf_op jit(solution)/shard_map/psum | solution.py:83
  24.5 12.2 %copy-start.3 = (f32[2,256]{1,0:T(2,128)S(1)}, f32[2,256]{1,0:T(2,128)}, u32[]{:S(2)}) copy-start(f32[2,256]{1,0:T(2,128)} %param.20) | copy-start | bytes 6148
  24.5 12.2 %copy-start.4 = (f32[2,128]{1,0:T(2,128)S(1)}, f32[2,128]{1,0:T(2,128)}, u32[]{:S(2)}) copy-start(f32[2,128]{1,0:T(2,128)} %param.21) | copy-start | bytes 3076
  24.5 12.3 %copy-start.8 = (u32[32]{0:T(128)S(1)}, u32[32]{0:T(128)}, u32[]{:S(2)}) copy-start(u32[32]{0:T(128)} %constant.51) | copy-start | bytes 388
  129.6 99.2 %reduce-scatter.21.cloned.1.call-start = ((), (), s32[]{:S(2)}) async-start(), calls=%async_computation.16 | async-start | bytes 81920 | tf_op jit(solution)/shard_map/reduce_scatter | solution.py:51
  133.9 3.9 copy-start.2
  140.6 68.1 %copy-start.6 = (bf16[2,1024,256]{2,1,0:T(8,128)(2,1)S(1)}, bf16[2,1024,256]{2,1,0:T(8,128)(2,1)}, u32[]{:S(2)}) copy-start(bf16[2,1024,256]{2,1,0:T(8,128)(2,1)} %param.15) | copy-start | bytes 3145732
  140.6 75.7 %copy-start.7 = (bf16[2,1024,256]{2,1,0:T(8,128)(2,1)S(1)}, bf16[2,1024,256]{2,1,0:T(8,128)(2,1)}, u32[]{:S(2)}) copy-start(bf16[2,1024,256]{2,1,0:T(8,128)(2,1)} %param.19) | copy-start | bytes 3145732
  209.6 41.2 %reduce-scatter.23.cloned.1.call-start = ((), (), s32[]{:S(2)}) async-start(), calls=%async_computation.17 | async-start | bytes 81920 | tf_op jit(solution)/shard_map/reduce_scatter | solution.py:51
  217.1 55.7 %reduce-scatter.25.cloned.1.call-start = ((), (), s32[]{:S(2)}) async-start(), calls=%async_computation.18 | async-start | bytes 81920 | tf_op jit(solution)/shard_map/reduce_scatter | solution.py:51
  219.1 76.2 %reduce-scatter.27.cloned.1.call-start = ((), (), s32[]{:S(2)}) async-start(), calls=%async_computation.19 | async-start | bytes 163840 | tf_op jit(solution)/shard_map/reduce_scatter | solution.py:51
  221.3 96.1 %reduce-scatter.29.cloned.1.call-start = ((), (), s32[]{:S(2)}) async-start(), calls=%async_computation.20 | async-start | bytes 163840 | tf_op jit(solution)/shard_map/reduce_scatter | solution.py:51
  223.6 173.4 %all-reduce.7.cloned.1.call-start = ((), (), s32[]{:S(2)}) async-start(), calls=%async_computation.21 | async-start | bytes 524288 | tf_op jit(solution)/shard_map/psum | solution.py:83
  325.8 4.0 copy-start
Sparse Core Ops, SparseCore 0:
  10.4 22.2 reduce-scatter.10
  35.1 19.5 reduce-scatter.12
  57.1 19.5 reduce-scatter.14
  79.6 19.6 reduce-scatter.16
  101.5 19.6 reduce-scatter.18
  129.8 70.9 all-reduce.4
  209.7 19.0 reduce-scatter.20
  231.2 19.5 reduce-scatter.22
  253.2 19.5 reduce-scatter.24
  275.6 19.6 reduce-scatter.26
  297.8 19.6 reduce-scatter.28
  326.0 71.0 all-reduce.6
where the time goes:
time: 414 us; the launch traced here: 412 us
  waiting for transfers between devices  278 us (67%)
  blocking collectives  36.8 us (9%)
  local copies, waits for them, and re-layouts  34.7 us (8%)
  matrix products  32.5 us (8%)
  between operations  15.1 us (4%)
  other arithmetic  14.5 us (4%)
    reduce_scatter x10, waiting for transfers between devices, local(): lax.psum_scatter(partials + (squares_part,), 'dp', scatter_dimension=0, t...  159 us
    psum x2, waiting for transfers between devices, local(): out_rows = lax.psum(partial_out, 'tp')  119 us
    dot_general x10, matrix products, local(): jnp.dot(normed, weights[section_index], preferred_element_type=jnp.float32)  16.9 us
    unnamed x2, blocking collectives  15 us
    another operation x4, local copies, waits for them, and re-layouts, local(): recurrent_state[section_index].reshape(local_seqs, value_cols, KEY)  14.9 us
    psum x2, blocking collectives, local(): out_squares = lax.psum(jnp.sum(out_rows * out_rows, axis=1), 'dp')  11.3 us
    dot_general x6, matrix products, spread_heads(): return jnp.einsum('bhk,hc->bck', shaped, spread, precision=highest)  11.2 us
    all_gather x2, blocking collectives, local(): lax.all_gather(mixed, 'dp', axis=0, tiled=True)  10.5 us
  transfers between devices with their start and end apart: 12, of which 11 were waited for; matrix products, arithmetic and copies ran while one was open for 16% of the time, Pallas kernels for 0%

commit v1 on v0

--- a/solution.py
+++ b/solution.py
@@ -80,7 +80,7 @@
             out_weight,
             preferred_element_type=jnp.float32,
         )
-        out_rows = lax.psum(partial_out, "tp")
+        out_rows = jnp.sum(lax.all_gather(partial_out, "tp"), axis=0)
         out_squares = lax.psum(jnp.sum(out_rows * out_rows, axis=1), "dp")
         residual = (
             wide_float

time: 414 us -> 369 us (0.89)
  waiting for transfers between devices: 278 us -> 234 us
    psum x2 -> x0, waiting for transfers between devices: 119 us -> none  [local(): out_rows = lax.psum(partial_out, 'tp')]
    all_gather x0 -> x2, waiting for transfers between devices: none -> 75.7 us  [local(): out_rows = jnp.sum(lax.all_gather(partial_out, 'tp'), axis=0)]
  transfers between devices with their start and end apart: 12 -> 12, of which waited for: 11 -> 11; matrix products, arithmetic and copies ran while one was open for 16% -> 18% of each run, Pallas kernels for 0% -> 0%
where the time goes in v1:
time: 369 us; the launch traced here: 367 us
  waiting for transfers between devices  234 us (63%)
  blocking collectives  36.8 us (10%)
  local copies, waits for them, and re-layouts  34.5 us (9%)
  matrix products  32.5 us (9%)
  between operations  15.1 us (4%)
  other arithmetic  14.2 us (4%)
    reduce_scatter x10, waiting for transfers between devices, local(): lax.psum_scatter(partials + (squares_part,), 'dp', scatter_dimension=0, t...  158 us
    all_gather x2, waiting for transfers between devices, local(): out_rows = jnp.sum(lax.all_gather(partial_out, 'tp'), axis=0)  75.7 us
    dot_general x10, matrix products, local(): jnp.dot(normed, weights[section_index], preferred_element_type=jnp.float32)  16.9 us
    unnamed x2, blocking collectives  15 us
    another operation x4, local copies, waits for them, and re-layouts, local(): recurrent_state[section_index].reshape(local_seqs, value_cols, KEY)  14.9 us
    psum x2, blocking collectives, local(): out_squares = lax.psum(jnp.sum(out_rows * out_rows, axis=1), 'dp')  11.3 us
    dot_general x6, matrix products, spread_heads(): return jnp.einsum('bhk,hc->bck', shaped, spread, precision=highest)  11.2 us
    all_gather x2, blocking collectives, local(): lax.all_gather(mixed, 'dp', axis=0, tiled=True)  10.5 us
  transfers between devices with their start and end apart: 12, of which 11 were waited for; matrix products, arithmetic and copies ran while one was open for 18% of the time, Pallas kernels for 0%

profile of v1, /device:TPU:0, one launch (start us, length us, event | category | flops | bytes accessed | tf_op | source)
XLA Modules:
  0.0 367.4 jit_solution(10581877750042106275)
XLA Ops:
  17.6 3.9 %fusion.83 = (f32[1,16,32768]{2,1,0:T(8,128)}, f32[1,16,32768]{2,1,0:T(8,128)S(1)}) fusion(f32[2,16,32768]{2,1,0:T(8,128)} %param.13), kind=kLoop, calls=%fused_computation.108 | loop fusion | bytes 8388608 | tf_op jit(solution)/shard_map/slice | solution.py:63
  21.5 3.0 reshape_squeeze.6
  24.5 3.8 %copy.18 = f32[16,512,64]{1,2,0:T(8,128)} copy(f32[16,512,64]{2,1,0:T(8,128)} %reshape_squeeze.6) | data formatting | bytes 4194304 | tf_op jit(solution)/shard_map/reshape;squeeze | solution.py:63
  28.3 8.4 %all-reduce = f32[64]{0:T(128)S(1)} all-reduce(f32[64]{0:T(128)S(1)} %fusion.41), channel_id=5, replica_groups=mesh['tp'=8,'dp'=4] {'dp'}, use_global_device_ids=true, to_apply=%region_2.3.clone | all-reduce | flops 64 | bytes 512
  38.1 16.7 %reduce-scatter.13.cloned.1.call-done = f32[16,256]{1,0:T(8,128)} async-done(((f32[64,256]{1,0:T(8,128)}), f32[16,256]{1,0:T(8,128)}) %reduce-scatter.13.cloned.1.call-update) | async-done | bytes 16400 | tf_op jit(solution)/shard_map/reduce_scatter | solution.py:51
  54.7 22.0 %reduce-scatter.15.cloned.1.call-done = f32[16,256]{1,0:T(8,128)} async-done(((f32[64,256]{1,0:T(8,128)}), f32[16,256]{1,0:T(8,128)}) %reduce-scatter.15.cloned.1.call-update) | async-done | bytes 16400 | tf_op jit(solution)/shard_map/reduce_scatter | solution.py:51
  77.8 2.4 fusion.79
  80.2 19.1 %reduce-scatter.17.cloned.1.call-done = f32[16,512]{1,0:T(8,128)} async-done(((f32[64,512]{1,0:T(8,128)}), f32[16,512]{1,0:T(8,128)}) %reduce-scatter.17.cloned.1.call-update) | async-done | bytes 32784 | tf_op jit(solution)/shard_map/reduce_scatter | solution.py:51
  100.1 2.7 fusion.2
  103.5 17.7 %reduce-scatter.19.cloned.1.call-done = f32[16,512]{1,0:T(8,128)} async-done(((f32[64,512]{1,0:T(8,128)}), f32[16,512]{1,0:T(8,128)}) %reduce-scatter.19.cloned.1.call-update) | async-done | bytes 32784 | tf_op jit(solution)/shard_map/reduce_scatter | solution.py:51
  122.2 5.2 %all_gather.18 = bf16[64,512]{1,0:T(8,128)(2,1)S(1)} all-gather(bf16[16,512]{1,0:T(8,128)(2,1)S(1)} %fusion.61), channel_id=1, replica_groups=mesh['tp'=8,'dp'=4] {'dp'}, dimensions={0}, use_global_device_ids=true | all-gather | bytes 81920 | tf_op jit(solution)/shard_map/all_gather | solution.py:79
  129.7 4.2 %reshape_squeeze.7 = f32[16,512,64]{2,1,0:T(8,128)} reshape(f32[1,16,32768]{2,1,0:T(8,128)} %get-tuple-element.4) | data formatting | bytes 4194304 | tf_op jit(solution)/shard_map/reshape;squeeze | solution.py:63
  133.9 3.8 %copy.19 = f32[16,512,64]{1,2,0:T(8,128)} copy(f32[16,512,64]{2,1,0:T(8,128)} %reshape_squeeze.7) | data formatting | bytes 4194304 | tf_op jit(solution)/shard_map/reshape;squeeze | solution.py:63
  137.8 2.8 copy.20
  140.5 3.9 %stack_reshape.6 = f32[1,16,32768]{2,1,0:T(8,128)} reshape(f32[16,512,64]{2,1,0:T(8,128)} %copy.20) | data formatting | bytes 4194304 | tf_op jit(solution)/shard_map/stack;reshape | solution.py:90
  144.5 34.4 %all-gather.5.cloned.1.call-done = f32[512,1024]{1,0:T(8,128)} async-done(((f32[64,1024]{1,0:T(8,128)}), f32[512,1024]{1,0:T(8,128)}) %all-gather.5.cloned.1.call-update) | async-done | bytes 2097168 | tf_op jit(solution)/shard_map/all_gather | solution.py:83
  180.8 5.7 %psum.14 = f32[64]{0:T(128)S(1)} all-reduce(f32[64]{0:T(128)S(1)} %multiply_reduce_fusion.1), channel_id=1, replica_groups=mesh['tp'=8,'dp'=4] {'dp'}, use_global_device_ids=true, to_apply=%region_11.12 | all-reduce | flops 64 | bytes 512 | tf_op jit(solution)/shard_map/psum | solution.py:84
  187.6 6.6 %all-reduce.1 = f32[64]{0:T(128)S(1)} all-reduce(f32[64]{0:T(128)S(1)} %get-tuple-element.2), channel_id=11, replica_groups=mesh['tp'=8,'dp'=4] {'dp'}, use_global_device_ids=true, to_apply=%region_14.15.clone | all-reduce | flops 64 | bytes 512
  201.6 4.4 %reduce-scatter.21.cloned.1.call-done = f32[16,256]{1,0:T(8,128)} async-done(((f32[64,256]{1,0:T(8,128)}), f32[16,256]{1,0:T(8,128)}) %reduce-scatter.21.cloned.1.call-update) | async-done | bytes 16400 | tf_op jit(solution)/shard_map/reduce_scatter | solution.py:51
  206.0 22.0 %reduce-scatter.23.cloned.1.call-done = f32[16,256]{1,0:T(8,128)} async-done(((f32[64,256]{1,0:T(8,128)}), f32[16,256]{1,0:T(8,128)}) %reduce-scatter.23.cloned.1.call-update) | async-done | bytes 16400 | tf_op jit(solution)/shard_map/reduce_scatter | solution.py:51
  228.0 22.0 %reduce-scatter.25.cloned.1.call-done = f32[16,256]{1,0:T(8,128)} async-done(((f32[64,256]{1,0:T(8,128)}), f32[16,256]{1,0:T(8,128)}) %reduce-scatter.25.cloned.1.call-update) | async-done | bytes 16400 | tf_op jit(solution)/shard_map/reduce_scatter | solution.py:51
  251.0 2.4 fusion.75
  253.5 19.0 %reduce-scatter.27.cloned.1.call-done = f32[16,512]{1,0:T(8,128)} async-done(((f32[64,512]{1,0:T(8,128)}), f32[16,512]{1,0:T(8,128)}) %reduce-scatter.27.cloned.1.call-update) | async-done | bytes 32784 | tf_op jit(solution)/shard_map/reduce_scatter | solution.py:51
  273.4 2.8 fusion
  276.6 2.8 copy.21
  279.5 15.1 %reduce-scatter.29.cloned.1.call-done = f32[16,512]{1,0:T(8,128)} async-done(((f32[64,512]{1,0:T(8,128)}), f32[16,512]{1,0:T(8,128)}) %reduce-scatter.29.cloned.1.call-update) | async-done | bytes 32784 | tf_op jit(solution)/shard_map/reduce_scatter | solution.py:51
  295.5 5.2 %all_gather.21 = bf16[64,512]{1,0:T(8,128)(2,1)S(1)} all-gather(bf16[16,512]{1,0:T(8,128)(2,1)S(1)} %fusion.58), channel_id=1, replica_groups=mesh['tp'=8,'dp'=4] {'dp'}, dimensions={0}, use_global_device_ids=true | all-gather | bytes 81920 | tf_op jit(solution)/shard_map/all_gather | solution.py:79
  300.8 2.2 fusion.4
  303.1 4.0 %stack_reshape.7 = f32[1,16,32768]{2,1,0:T(8,128)} reshape(f32[16,512,64]{2,1,0:T(8,128)} %copy.21) | data formatting | bytes 4194304 | tf_op jit(solution)/shard_map/stack;reshape | solution.py:90
  307.1 3.9 %pad_maximum_fusion = f32[2,16,32768]{2,1,0:T(8,128)} fusion(f32[1,16,32768]{2,1,0:T(8,128)} %stack_reshape.7, f32[1,16,32768]{2,1,0:T(8,128)S(1)} %copy-done), kind=kLoop, calls=%fused_computation | loop fusion | flops 1048576 | bytes 8388608 | tf_op jit(solution)/shard_map/stack | solution.py:90
  311.0 41.3 %all-gather.7.cloned.1.call-done = f32[512,1024]{1,0:T(8,128)} async-done(((f32[64,1024]{1,0:T(8,128)}), f32[512,1024]{1,0:T(8,128)}) %all-gather.7.cloned.1.call-update) | async-done | bytes 2097168 | tf_op jit(solution)/shard_map/all_gather | solution.py:83
  354.2 5.7 %psum.15 = f32[64]{0:T(128)S(1)} all-reduce(f32[64]{0:T(128)S(1)} %multiply_reduce_fusion), channel_id=1, replica_groups=mesh['tp'=8,'dp'=4] {'dp'}, use_global_device_ids=true, to_apply=%region_23.24 | all-reduce | flops 64 | bytes 512 | tf_op jit(solution)/shard_map/psum | solution.py:84
  (97 shorter events, 33.3 us)
Async XLA Ops:
  7.2 7.0 %copy-start.1 = (bf16[64,1024]{1,0:T(8,128)(2,1)S(1)}, bf16[64,1024]{1,0:T(8,128)(2,1)}, u32[]{:S(2)}) copy-start(bf16[64,1024]{1,0:T(8,128)(2,1)} %param.12) | copy-start | bytes 393220
  7.2 7.0 %copy-start.5 = (bf16[2,1024,512]{2,1,0:T(8,128)(2,1)S(1)}, bf16[2,1024,512]{2,1,0:T(8,128)(2,1)}, u32[]{:S(2)}) copy-start(bf16[2,1024,512]{2,1,0:T(8,128)(2,1)} %param.17) | copy-start | bytes 6291460
  7.2 30.9 %reduce-scatter.11.cloned.1.call-start = ((), (), s32[]{:S(2)}) async-start(), calls=%async_computation.10 | async-start | bytes 81920 | tf_op jit(solution)/shard_map/reduce_scatter | solution.py:51
  10.1 44.6 %reduce-scatter.13.cloned.1.call-start = ((), (), s32[]{:S(2)}) async-start(), calls=%async_computation.11 | async-start | bytes 81920 | tf_op jit(solution)/shard_map/reduce_scatter | solution.py:51
  12.1 64.6 %reduce-scatter.15.cloned.1.call-start = ((), (), s32[]{:S(2)}) async-start(), calls=%async_computation.12 | async-start | bytes 81920 | tf_op jit(solution)/shard_map/reduce_scatter | solution.py:51
  14.1 85.1 %reduce-scatter.17.cloned.1.call-start = ((), (), s32[]{:S(2)}) async-start(), calls=%async_computation.13 | async-start | bytes 163840 | tf_op jit(solution)/shard_map/reduce_scatter | solution.py:51
  15.2 106.0 %reduce-scatter.19.cloned.1.call-start = ((), (), s32[]{:S(2)}) async-start(), calls=%async_computation.14 | async-start | bytes 163840 | tf_op jit(solution)/shard_map/reduce_scatter | solution.py:51
  17.4 161.5 %all-gather.5.cloned.1.call-start = ((), (), s32[]{:S(2)}) async-start(), calls=%async_computation.20 | async-start | bytes 2359296 | tf_op jit(solution)/shard_map/all_gather | solution.py:83
  24.5 12.2 %copy-start.3 = (f32[2,256]{1,0:T(2,128)S(1)}, f32[2,256]{1,0:T(2,128)}, u32[]{:S(2)}) copy-start(f32[2,256]{1,0:T(2,128)} %param.20) | copy-start | bytes 6148
  24.5 12.2 %copy-start.4 = (f32[2,128]{1,0:T(2,128)S(1)}, f32[2,128]{1,0:T(2,128)}, u32[]{:S(2)}) copy-start(f32[2,128]{1,0:T(2,128)} %param.21) | copy-start | bytes 3076
  24.5 12.3 %copy-start.8 = (u32[32]{0:T(128)S(1)}, u32[32]{0:T(128)}, u32[]{:S(2)}) copy-start(u32[32]{0:T(128)} %constant.51) | copy-start | bytes 388
  129.6 76.4 %reduce-scatter.21.cloned.1.call-start = ((), (), s32[]{:S(2)}) async-start(), calls=%async_computation.15 | async-start | bytes 81920 | tf_op jit(solution)/shard_map/reduce_scatter | solution.py:51
  133.9 3.8 %copy-start.2 = (f32[2,1024]{1,0:T(2,128)S(1)}, f32[2,1024]{1,0:T(2,128)}, u32[]{:S(2)}) copy-start(f32[2,1024]{1,0:T(2,128)} %param.23) | copy-start | bytes 24580
  144.4 42.2 %copy-start.6 = (bf16[2,1024,256]{2,1,0:T(8,128)(2,1)S(1)}, bf16[2,1024,256]{2,1,0:T(8,128)(2,1)}, u32[]{:S(2)}) copy-start(bf16[2,1024,256]{2,1,0:T(8,128)(2,1)} %param.15) | copy-start | bytes 3145732
  144.5 49.7 %copy-start.7 = (bf16[2,1024,256]{2,1,0:T(8,128)(2,1)S(1)}, bf16[2,1024,256]{2,1,0:T(8,128)(2,1)}, u32[]{:S(2)}) copy-start(bf16[2,1024,256]{2,1,0:T(8,128)(2,1)} %param.19) | copy-start | bytes 3145732
  187.5 40.5 %reduce-scatter.23.cloned.1.call-start = ((), (), s32[]{:S(2)}) async-start(), calls=%async_computation.16 | async-start | bytes 81920 | tf_op jit(solution)/shard_map/reduce_scatter | solution.py:51
  195.1 55.0 %reduce-scatter.25.cloned.1.call-start = ((), (), s32[]{:S(2)}) async-start(), calls=%async_computation.17 | async-start | bytes 81920 | tf_op jit(solution)/shard_map/reduce_scatter | solution.py:51
  197.0 75.5 %reduce-scatter.27.cloned.1.call-start = ((), (), s32[]{:S(2)}) async-start(), calls=%async_computation.18 | async-start | bytes 163840 | tf_op jit(solution)/shard_map/reduce_scatter | solution.py:51
  199.3 95.4 %reduce-scatter.29.cloned.1.call-start = ((), (), s32[]{:S(2)}) async-start(), calls=%async_computation.19 | async-start | bytes 163840 | tf_op jit(solution)/shard_map/reduce_scatter | solution.py:51
  201.6 150.7 %all-gather.7.cloned.1.call-start = ((), (), s32[]{:S(2)}) async-start(), calls=%async_computation.21 | async-start | bytes 2359296 | tf_op jit(solution)/shard_map/all_gather | solution.py:83
  303.0 4.1 %copy-start = (f32[1,16,32768]{2,1,0:T(8,128)S(1)}, f32[1,16,32768]{2,1,0:T(8,128)}, u32[]{:S(2)}) copy-start(f32[1,16,32768]{2,1,0:T(8,128)} %stack_reshape.6) | copy-start | bytes 6291460
Sparse Core Ops, SparseCore 0:
  10.4 22.2 reduce-scatter.10
  35.1 19.5 reduce-scatter.12
  57.1 19.5 reduce-scatter.14
  79.6 19.6 reduce-scatter.16
  101.5 19.6 reduce-scatter.18
  129.8 49.0 all-gather.4
  187.7 18.3 reduce-scatter.20
  208.4 19.5 reduce-scatter.22
  230.5 19.5 reduce-scatter.24
  252.9 19.6 reduce-scatter.26
  275.0 19.6 reduce-scatter.28
  303.2 49.0 all-gather.6
